TPU v7x, 32 devices: a whole 2x2x4 slice. The times are simulated.
32 devices in a mesh: sp: 8 (over z, x), tp: 4 (over y, core).
Axes of the slice: x: 2, y: 2, z: 4, core: 2. Of those that a mesh axis runs over, the one named last changes fastest.
Arguments:
- query_logits: bfloat16 [4096, 4096], P('sp', 'tp'), may hold values from -6 to 6
- forget_logits: bfloat16 [4096, 4096], P('sp', 'tp'), may hold values from -6 to 6
- value_inputs: bfloat16 [4096, 4096], P('sp', 'tp'), may hold values from -16 to 16
- output_gate_logits: bfloat16 [4096, 4096], P('sp', 'tp'), may hold values from -6 to 6
- forget_floor_gap: float32 [4096], replicated, may hold values from 2.4414063e-05 to 0.1
- surge_log_decay: float32 [32, 4096], P('tp', 'sp'), may hold values from -0.7 to 0
- head_norm_gain: float32 [128], replicated, may hold values from 0.1 to 1.9
- output_matrix: bfloat16 [4096, 4096], P('sp', 'tp'), may hold values from -1.25 to 1.25
- branch_norm_gain: float32 [4096], replicated, may hold values from 0.1 to 1.9
- residual: bfloat16 [4096, 4096], P('sp', 'tp'), may hold values from -6 to 6
Outputs:
- output: bfloat16 [4096, 4096], P('sp', 'tp')
All inputs are finite; a program needn't handle non-finite values.
Results may differ from a plain program's by a relative error of at most 0.005.
Values may be sent and summed in bfloat16 or wider, within the bound.
No kernel may reach another device: no remote copies, remote signals or barrier semaphores. Data moves between devices by JAX's collectives and lax.ppermute only.
A program may use at most 128 MiB of HBM per device.

v0:
```python
import jax
import jax.numpy as jnp
from jax import lax
from jax.sharding import PartitionSpec as P

HEAD_DIM = 128
D = 4096
BLOCK_SPAN = 64
epsilon = 1e-06


def prefix(shard, axis, combine, identity):
    size, position = (lax.axis_size(axis), lax.axis_index(axis))
    everything = jax.tree.map(lambda part: lax.all_gather(part, axis), shard)
    start = jax.tree.map(
        lambda part, zero: jnp.broadcast_to(jnp.asarray(zero, part.dtype), part.shape),
        shard,
        identity,
    )

    def step(k, before):
        reached = k < position
        new = combine(before, jax.tree.map(lambda part: part[k], everything))
        return jax.tree.map(lambda a, b: jnp.where(reached, a, b), new, before)

    return lax.fori_loop(0, size, step, start)


def block_update(state, queries, keys_in, values_in, running):
    length = running.shape[1]
    middle = length // 2
    anchor = running[:, middle - 1 : middle, :]
    ending = running[:, -1:, :]
    causal = jnp.tril(jnp.ones((length, length), dtype=bool))
    highest = lax.Precision.HIGHEST
    inter = jnp.einsum("htd,hde->hte", queries * jnp.exp(running), state, precision=highest)
    scores = jnp.einsum(
        "htd,hsd->hts",
        queries * jnp.exp(running - anchor),
        keys_in * jnp.exp(anchor - running),
        precision=highest,
    )
    intra = jnp.einsum(
        "hts,hse->hte", jnp.where(causal[None], scores, 0.0), values_in, precision=highest
    )
    new_state = state * jnp.exp(ending[:, 0, :])[:, :, None] + jnp.einsum(
        "hsd,hse->hde", keys_in * jnp.exp(ending - running), values_in, precision=highest
    )
    return (new_state, inter + intra)


def head_gates(query_logits, forget_logits, value_inputs, gap):
    row_count = query_logits.shape[0]
    head_count = query_logits.shape[1] // HEAD_DIM

    def shaped(array):
        return array.astype(jnp.float32).reshape(row_count, head_count, HEAD_DIM)

    queries = jax.nn.silu(shaped(query_logits)) * HEAD_DIM ** (-0.5)
    keys_in = gap.reshape(head_count, HEAD_DIM) * jax.nn.sigmoid(-shaped(forget_logits))
    values_in = shaped(value_inputs)
    decay_factors = jnp.log1p(-keys_in)
    return (queries, keys_in, values_in, decay_factors)


def gated_norm(heads_out, output_gate_logits, head_norm_gain):
    mean_sq = jnp.mean(heads_out * heads_out, axis=-1, keepdims=True)
    gates = jax.nn.silu(output_gate_logits.astype(jnp.float32).reshape(heads_out.shape))
    normed = heads_out * lax.rsqrt(mean_sq + epsilon) * head_norm_gain * gates
    return normed.reshape(heads_out.shape[0], -1).astype(jnp.bfloat16)


def combine(earlier, later):
    return (earlier[0] * later[0], later[0][:, :, None] * earlier[1] + later[1])


def per_device(
    query_logits,
    forget_logits,
    value_inputs,
    output_gate_logits,
    forget_floor_gap,
    surge_log_decay,
    head_norm_gain,
    output_matrix,
    branch_norm_gain,
    residual,
):
    row_count = query_logits.shape[0]
    head_cols = query_logits.shape[1]
    head_count = head_cols // HEAD_DIM
    number_of_blocks = row_count // BLOCK_SPAN
    column = lax.axis_index("tp")
    whole_weight = lax.all_gather(output_matrix, "sp", axis=0, tiled=True)
    gap = lax.dynamic_slice_in_dim(forget_floor_gap, column * head_cols, head_cols)
    queries, keys_in, values_in, decay_factors = head_gates(
        query_logits, forget_logits, value_inputs, gap
    )
    decay_factors = decay_factors + jnp.transpose(surge_log_decay)[:, :, None]

    def to_blocks(array):
        return array.reshape(number_of_blocks, BLOCK_SPAN, head_count, HEAD_DIM).transpose(
            0, 2, 1, 3
        )

    queries = to_blocks(queries)
    running = jnp.cumsum(to_blocks(decay_factors), axis=2)

    def step_forward(state, input_tuple):
        return block_update(state, input_tuple[0], input_tuple[1], input_tuple[2], input_tuple[3])

    starting_state = jnp.zeros((head_count, HEAD_DIM, HEAD_DIM), jnp.float32)
    end_state, local_out = lax.scan(
        step_forward, starting_state, (queries, to_blocks(keys_in), to_blocks(values_in), running)
    )
    totals = running[:, :, -1, :]
    before = jnp.cumsum(totals, axis=0) - totals
    whole_decay = jnp.exp(jnp.sum(totals, axis=0))
    identity = (jnp.ones_like(whole_decay), jnp.zeros_like(end_state))
    unused_slot, carried = prefix((whole_decay, end_state), "sp", combine, identity)
    reach = queries * jnp.exp(running + before[:, :, None, :])
    heads_out = local_out + jnp.einsum(
        "nhtd,hde->nhte", reach, carried, precision=lax.Precision.HIGHEST
    )
    heads_out = heads_out.transpose(0, 2, 1, 3).reshape(row_count, head_count, HEAD_DIM)
    mixed_rows = gated_norm(heads_out, output_gate_logits, head_norm_gain)
    all_heads = lax.all_gather(mixed_rows, "tp", axis=1, tiled=True)
    projected = jnp.dot(all_heads, whole_weight, preferred_element_type=jnp.float32)
    branch = lax.optimization_barrier(projected.astype(jnp.bfloat16)).astype(jnp.float32)
    squares = lax.psum(jnp.sum(branch * branch, axis=1), "tp")
    scale = lax.rsqrt(squares / D + epsilon)
    out_cols = branch.shape[1]
    gain_part = lax.dynamic_slice_in_dim(branch_norm_gain, column * out_cols, out_cols)
    return (residual.astype(jnp.float32) + branch * scale[:, None] * gain_part).astype(jnp.bfloat16)


def solution(mesh):
    placed = (
        P("sp", "tp"),
        P("sp", "tp"),
        P("sp", "tp"),
        P("sp", "tp"),
        P(),
        P("tp", "sp"),
        P(),
        P("sp", "tp"),
        P(),
        P("sp", "tp"),
    )
    return jax.shard_map(
        per_device, mesh=mesh, in_specs=placed, out_specs=P("sp", "tp"), check_vma=False
    )
```

profile of v0, /device:TPU:0, one launch (start us, length us, event | category | flops | bytes accessed | tf_op | source)
XLA Modules:
  0.0 348.8 jit_solution(4762647425927424889)
XLA Ops:
  6.5 0.8 copy.35
  7.4 1.8 divide_bitcast_fusion
  9.2 1.8 copy.48
  11.7 0.7 copy-done.4
  13.2 1.5 bitcast_bitcast_fusion
  14.6 4.0 %fusion.36 = f32[8,8,64,128]{3,1,2,0:T(8,128)} fusion(f32[8,64,8]{2,1,0:T(8,128)S(1)} %bitcast.184, f32[8,128]{1,0:T(8,128)S(1)} %dynamic-slice_bitcast_fusion.1, f32[8,64,8,128]{3,2,1,0:T(8,128)} %bitcast.177), kind=kOutput, calls=%fused_computation.60 | output fusion | flops 34603008 | bytes 4214784 | tf_op jit(solution)/shard_map/jit(cumsum)/reduce_window_sum | solution.py:107
  18.6 2.5 fusion.34
  21.1 47.1 %while.27 = (s32[]{:T(128)}, f32[8,128,128]{2,1,0:T(8,128)S(1)}, f32[8,8,64,128]{3,2,0,1:T(8,128)}, f32[8,8,64,128]{3,1,2,0:T(8,128)}, f32[8,8,64,128]{3,1,2,0:T...) while((s32[]{:T(128)}, f32[8,128,128]{2,1,0:T(8,128)S(1)}, ...), condition=%wide.region_2.3_spmd.clone, body=%wide.region_1.2_spmd.clone.sunk | while | flops 303075328 | bytes 7647356 | solution.py:113
  21.1 1.1 constant_dynamic-slice_fusion.7
  22.2 1.1 constant_dynamic-slice_fusion.6
  24.1 1.2 convolution_add_fusion.3
  25.9 1.1 fusion.74
  27.0 1.1 constant_dynamic-slice_fusion.7
  28.1 1.1 constant_dynamic-slice_fusion.6
  29.9 1.2 convolution_add_fusion.3
  31.8 1.1 fusion.74
  32.9 1.1 constant_dynamic-slice_fusion.7
  34.0 1.1 constant_dynamic-slice_fusion.6
  35.8 1.2 convolution_add_fusion.3
  37.7 1.1 fusion.74
  38.8 1.1 constant_dynamic-slice_fusion.7
  39.9 1.1 constant_dynamic-slice_fusion.6
  41.7 1.2 convolution_add_fusion.3
  43.5 1.2 fusion.74
  44.7 1.1 constant_dynamic-slice_fusion.7
  45.8 1.1 constant_dynamic-slice_fusion.6
  47.6 1.2 convolution_add_fusion.3
  49.5 1.1 fusion.74
  50.6 1.1 constant_dynamic-slice_fusion.7
  51.7 1.1 constant_dynamic-slice_fusion.6
  53.5 1.2 convolution_add_fusion.3
  55.3 1.1 fusion.74
  56.4 1.1 constant_dynamic-slice_fusion.7
  57.5 1.1 constant_dynamic-slice_fusion.6
  59.3 1.2 convolution_add_fusion.3
  61.2 1.2 fusion.74
  62.3 1.1 constant_dynamic-slice_fusion.7
  63.4 1.1 constant_dynamic-slice_fusion.6
  65.2 1.2 convolution_add_fusion.3
  67.1 1.1 fusion.74
  68.2 0.8 copy-done.1
  69.1 0.8 slice_reduce_fusion
  69.9 33.1 %all-gather = f32[64,128]{1,0:T(8,128)S(1)} all-gather(f32[8,128]{1,0:T(8,128)S(1)} %exp.52), channel_id=2, replica_groups=mesh['sp'=8,'tp'=4] {'sp'}, dimensions={0}, use_global_device_ids=true | all-gather | bytes 36864 | tf_op jit(solution)/shard_map/all_gather | solution.py:14
  103.0 0.9 fusion.47
  103.9 3.8 %exponential_multiply_fusion = f32[8,8,64,128]{3,1,2,0:T(8,128)} fusion(f32[8,8,64,128]{3,1,2,0:T(8,128)} %get-tuple-element.376, f32[8,8,128]{2,1,0:T(8,128)S(1)} %fusion.47, f32[8,64,8,128]{3,2,1,0:T(8,128)S(1)} %bitcast.176), kind=kLoop, calls=%fused_computation.67 | loop fusion | flops 3670016 | bytes 6324224 | tf_op jit(solution)/shard_map/mul | solution.py:121
  107.7 37.2 %all-gather.10.cloned.1.call-done = f32[64,128,128]{2,1,0:T(8,128)} async-done(((f32[8,128,128]{2,1,0:T(8,128)}), f32[64,128,128]{2,1,0:T(8,128)}) %all-gather.10.cloned.1.call-update) | async-done | bytes 4194320 | tf_op jit(solution)/shard_map/all_gather | solution.py:14
  144.9 11.4 %while.28 = (s32[]{:T(128)}, f32[8,128,128]{2,1,0:T(8,128)S(1)}, s32[]{:T(128)}, f32[8,8,128]{2,1,0:T(8,128)S(1)}, f32[8,8,128,128]{3,2,1,0:T(8,128)}, /*index=5*/s32[]{:T(128)}, s32[]{:T(128)}) while((s32[]{:T(128)}, f32[8,128,128]{2,1,0:T(8,128)S(1)}, s32[]{:T(128)}, f32[8,8,128]{2,1,0:T(8,128)S(1)}, ...), condition=%wide.region_5.6_spmd.clone, body=%wide.region_4.5_spmd.clone.sunk | while | flops 524292 | bytes 1585265 | solution.py:26
  144.9 1.4 fusion.75
  146.3 1.4 fusion.75
  147.8 1.4 fusion.75
  149.2 1.4 fusion.75
  150.6 1.4 fusion.75
  152.0 1.4 fusion.75
  153.5 1.4 fusion.75
  154.9 1.4 fusion.75
  156.3 4.7 %multiply_reduce_fusion = (f32[8,64,8]{1,0,2:T(8,128)S(1)}, f32[8,64,8,128]{3,1,0,2:T(8,128)S(1)}) fusion(f32[8,8,64,128]{3,2,0,1:T(8,128)} %get-tuple-element.137, f32[8,8,64,128]{3,1,2,0:T(8,128)} %exponential_multiply_fusion, f32[8,128,128]{2,1,0:T(8,128)S(1)} %get-tuple-element.139), kind=kOutput, calls=%fused_computation.66 | convolution fusion | flops 806875136 | bytes 6832128 | tf_op jit(solution)/shard_map/nhtd,hde->nhte/dot_general | solution.py:122
  161.1 1.2 copy.32
  163.5 2.2 fusion.43
  165.9 0.7 all-gather.8.cloned.1.call-update
  166.6 32.4 %all-gather.6.cloned.1.call-done = bf16[512,4096]{1,0:T(8,128)(2,1)} async-done(((bf16[512,1024]{1,0:T(8,128)(2,1)}), bf16[512,4096]{1,0:T(8,128)(2,1)}) %all-gather.6.cloned.1.call-update) | async-done | bytes 4194320 | tf_op jit(solution)/shard_map/all_gather | solution.py:127
  199.0 126.6 %all-gather.8.cloned.1.call-done = bf16[4096,1024]{1,0:T(8,128)(2,1)} async-done(((bf16[512,1024]{1,0:T(8,128)(2,1)}), bf16[4096,1024]{1,0:T(8,128)(2,1)}) %all-gather.8.cloned.1.call-update) | async-done | bytes 8388624 | tf_op jit(solution)/shard_map/all_gather | solution.py:94
  325.6 9.1 %convolution_convert_fusion = bf16[512,1024]{1,0:T(8,128)(2,1)S(1)} fusion(bf16[512,4096]{1,0:T(8,128)(2,1)} %all-gather.6.cloned.1.call-done, bf16[4096,1024]{1,0:T(8,128)(2,1)} %all-gather.8.cloned.1.call-done), kind=kOutput, calls=%fused_computation.74 | convolution fusion | flops 4295491584 | bytes 13631488 | tf_op jit(solution)/shard_map/dot_general | solution.py:128
  335.0 5.9 %psum.7 = f32[512]{0:T(512)S(1)} all-reduce(f32[512]{0:T(512)S(1)} %fusion.25), channel_id=1, replica_groups=mesh['sp'=8,'tp'=4] {'tp'}, use_global_device_ids=true, to_apply=%region_9.10 | all-reduce | flops 512 | bytes 4096 | tf_op jit(solution)/shard_map/psum | solution.py:130
  340.9 1.4 fusion.28
  (92 shorter events, 14.4 us)
Async XLA Ops:
  6.5 8.1 %copy-start = (f32[4096]{0:T(1024)S(1)}, f32[4096]{0:T(1024)}, u32[]{:S(2)}) copy-start(f32[4096]{0:T(1024)} %param.18) | copy-start | bytes 49156
  6.5 138.4 %all-gather.10.cloned.1.call-start = ((), (), s32[]{:S(2)}) async-start(), calls=%async_computation.2 | async-start | bytes 4718592 | tf_op jit(solution)/shard_map/all_gather | solution.py:14
  9.2 1.8 copy-start.3
  11.2 1.2 copy-start.4
  14.6 4.0 %copy-start.2 = (f32[64,8,8,128]{3,2,1,0:T(8,128)S(1)}, f32[64,8,8,128]{3,2,1,0:T(8,128)}, u32[]{:S(2)}) copy-start(f32[64,8,8,128]{3,2,1,0:T(8,128)} %copy.48) | copy-start | bytes 6291460
  21.1 81.9 %copy-start.7 = (f32[128]{0:T(128)S(1)}, f32[128]{0:T(128)}, u32[]{:S(2)}) copy-start(f32[128]{0:T(128)} %param.20) | copy-start | bytes 1540
  68.2 0.8 copy-start.1
  69.0 129.9 %all-gather.6.cloned.1.call-start = ((), (), s32[]{:S(2)}) async-start(), calls=%async_computation | async-start | bytes 5242880 | tf_op jit(solution)/shard_map/all_gather | solution.py:127
  162.3 1.2 copy-start.6
  165.8 159.8 %all-gather.8.cloned.1.call-start = ((), (), s32[]{:S(2)}) async-start(), calls=%async_computation.1 | async-start | bytes 9437184 | tf_op jit(solution)/shard_map/all_gather | solution.py:94
  166.5 174.3 %copy-start.5 = (bf16[512,1024]{1,0:T(8,128)(2,1)S(1)}, bf16[512,1024]{1,0:T(8,128)(2,1)}, u32[]{:S(2)}) copy-start(bf16[512,1024]{1,0:T(8,128)(2,1)} %param.23) | copy-start | bytes 3145732
  166.6 174.3 %dynamic-slice-start = ((f32[4096]{0:T(1024)}, s32[]{:T(128)}), f32[1024]{0:T(1024)S(1)}, s32[]{:S(2)}) async-start(f32[4096]{0:T(1024)} %param.22, s32[]{:T(128)} %select_n.32), calls=%async_computation.3 | async-start | bytes 8704 | tf_op jit(solution)/shard_map/dynamic_slice | solution.py:133
Sparse Core Ops, SparseCore 0:
  69.2 75.6 all-gather.9
  165.9 32.9 all-gather.5
  201.1 124.4 all-gather.7
where the time goes:
time: 350 us; the launch traced here: 349 us
  waiting for transfers between devices  197 us (56%)
  matrix products  42.7 us (12%)
  blocking collectives  39 us (11%)
  other arithmetic  29.2 us (8%)
  local copies, waits for them, and re-layouts  26.9 us (8%)
  between operations  13.3 us (4%)
    all_gather x1, waiting for transfers between devices, per_device(): whole_weight = lax.all_gather(output_matrix, 'sp', axis=0, tiled=True)  127 us
    all_gather x1, waiting for transfers between devices, prefix(): everything = jax.tree.map(lambda part: lax.all_gather(part, axis), shard)  37.2 us
    all_gather x1, blocking collectives, prefix(): everything = jax.tree.map(lambda part: lax.all_gather(part, axis), shard)  33.1 us
    all_gather x1, waiting for transfers between devices, per_device(): all_heads = lax.all_gather(mixed_rows, 'tp', axis=1, tiled=True)  32.4 us
    dynamic_slice x24, local copies, waits for them, and re-layouts, per_device(): lax.scan(step_forward, starting_state, (queries, to_blocks(keys_in), to_b...  17.5 us
    select_n x8, other arithmetic, step(): return jax.tree.map(lambda a, b: jnp.where(reached, a, b), new, before)  11 us
    dot_general x8, matrix products, block_update(): jnp.einsum('hsd,hse->hde', keys_in * jnp.exp(ending - running), values_in...  9.24 us
    dot_general x1, matrix products, per_device(): jnp.dot(all_heads, whole_weight, preferred_element_type=jnp.float32)  9.14 us
  transfers between devices with their start and end apart: 3, of which 3 were waited for; matrix products, arithmetic and copies ran while one was open for 2% of the time, Pallas kernels for 0%

commit v1 on v0

--- a/solution.py
+++ b/solution.py
@@ -124,7 +124,12 @@
     )
     heads_out = heads_out.transpose(0, 2, 1, 3).reshape(row_count, head_count, HEAD_DIM)
     mixed_rows = gated_norm(heads_out, output_gate_logits, head_norm_gain)
-    all_heads = lax.all_gather(mixed_rows, "tp", axis=1, tiled=True)
+    ring = [mixed_rows]
+    for hop in range(3):
+        ring.append(lax.ppermute(ring[-1], "tp", [(dev, (dev + 1) % 4) for dev in range(4)]))
+    all_heads = jnp.roll(
+        jnp.concatenate(ring[::-1], axis=1), (lax.axis_index("tp") + 1) * ring[0].shape[1], axis=1
+    )
     projected = jnp.dot(all_heads, whole_weight, preferred_element_type=jnp.float32)
     branch = lax.optimization_barrier(projected.astype(jnp.bfloat16)).astype(jnp.float32)
     squares = lax.psum(jnp.sum(branch * branch, axis=1), "tp")

time: 350 us -> 294 us (0.84)
  waiting for transfers between devices: 197 us -> 130 us
  local copies, waits for them, and re-layouts: 26.9 us -> 38.9 us
    all_gather x1, waiting for transfers between devices: 127 us -> 49.5 us  [per_device(): whole_weight = lax.all_gather(output_matrix, 'sp', axis=0, tiled=True)]
    ppermute x0 -> x3, waiting for transfers between devices: none -> 42.8 us  [per_device(): lax.ppermute(ring[-1], 'tp', [(dev, (dev + 1) % 4) for dev in range(4)])]
    all_gather x1 -> x0, waiting for transfers between devices: 32.4 us -> none  [per_device(): all_heads = lax.all_gather(mixed_rows, 'tp', axis=1, tiled=True)]
    unnamed x19 -> x32, local copies, waits for them, and re-layouts: 4.89 us -> 15 us
  transfers between devices with their start and end apart: 3 -> 5, of which waited for: 3 -> 5; matrix products, arithmetic and copies ran while one was open for 2% -> 13% of each run, Pallas kernels for 0% -> 0%
where the time goes in v1:
time: 294 us; the launch traced here: 293 us
  waiting for transfers between devices  130 us (44%)
  matrix products  42.5 us (14%)
  blocking collectives  39 us (13%)
  local copies, waits for them, and re-layouts  38.9 us (13%)
  other arithmetic  28.4 us (10%)
  between operations  13.6 us (5%)
    all_gather x1, waiting for transfers between devices, per_device(): whole_weight = lax.all_gather(output_matrix, 'sp', axis=0, tiled=True)  49.5 us
    ppermute x3, waiting for transfers between devices, per_device(): lax.ppermute(ring[-1], 'tp', [(dev, (dev + 1) % 4) for dev in range(4)])  42.8 us
    all_gather x1, waiting for transfers between devices, prefix(): everything = jax.tree.map(lambda part: lax.all_gather(part, axis), shard)  36.7 us
    all_gather x1, blocking collectives, prefix(): everything = jax.tree.map(lambda part: lax.all_gather(part, axis), shard)  33.1 us
    dynamic_slice x24, local copies, waits for them, and re-layouts, per_device(): lax.scan(step_forward, starting_state, (queries, to_blocks(keys_in), to_b...  17.6 us
    unnamed x32, local copies, waits for them, and re-layouts  15 us
    select_n x8, other arithmetic, step(): return jax.tree.map(lambda a, b: jnp.where(reached, a, b), new, before)  11.3 us
    dot_general x8, matrix products, block_update(): jnp.einsum('hsd,hse->hde', keys_in * jnp.exp(ending - running), values_in...  9.25 us
  transfers between devices with their start and end apart: 5, of which 5 were waited for; matrix products, arithmetic and copies ran while one was open for 13% of the time, Pallas kernels for 0%

profile of v1, /device:TPU:0, one launch (start us, length us, event | category | flops | bytes accessed | tf_op | source)
XLA Modules:
  0.0 292.9 jit_solution(11331765830208278709)
XLA Ops:
  6.5 1.8 divide_bitcast_fusion
  8.4 1.8 copy.48
  12.5 1.5 bitcast_bitcast_fusion
  14.0 3.9 %fusion.38 = f32[8,8,64,128]{3,1,2,0:T(8,128)} fusion(f32[8,64,8]{2,1,0:T(8,128)S(1)} %bitcast.183, f32[8,128]{1,0:T(8,128)S(1)} %dynamic-slice_bitcast_fusion.1, f32[8,64,8,128]{3,2,1,0:T(8,128)} %bitcast.176), kind=kOutput, calls=%fused_computation.62 | output fusion | flops 34603008 | bytes 4214784 | tf_op jit(solution)/shard_map/jit(cumsum)/reduce_window_sum | solution.py:107
  17.9 2.6 fusion.36
  20.5 47.0 %while.27 = (s32[]{:T(128)}, f32[8,128,128]{2,1,0:T(8,128)S(1)}, f32[8,8,64,128]{3,2,0,1:T(8,128)}, f32[8,8,64,128]{3,1,2,0:T(8,128)}, f32[8,8,64,128]{3,1,2,0:T...) while((s32[]{:T(128)}, f32[8,128,128]{2,1,0:T(8,128)S(1)}, ...), condition=%wide.region_2.3_spmd.clone, body=%wide.region_1.2_spmd.clone.sunk | while | flops 303075328 | bytes 7647856 | solution.py:113
  20.5 1.1 constant_dynamic-slice_fusion.6
  21.7 1.1 constant_dynamic-slice_fusion.7
  24.1 1.1 fusion.79
  25.2 1.2 convolution_add_fusion.3
  26.4 1.1 constant_dynamic-slice_fusion.6
  27.5 1.1 constant_dynamic-slice_fusion.7
  30.0 1.1 fusion.79
  31.1 1.2 convolution_add_fusion.3
  32.3 1.1 constant_dynamic-slice_fusion.6
  33.4 1.1 constant_dynamic-slice_fusion.7
  35.9 1.1 fusion.79
  37.0 1.2 convolution_add_fusion.3
  38.1 1.1 constant_dynamic-slice_fusion.6
  39.3 1.1 constant_dynamic-slice_fusion.7
  41.7 1.1 fusion.79
  42.9 1.2 convolution_add_fusion.3
  44.0 1.1 constant_dynamic-slice_fusion.6
  45.2 1.1 constant_dynamic-slice_fusion.7
  47.6 1.1 fusion.79
  48.7 1.2 convolution_add_fusion.3
  49.9 1.1 constant_dynamic-slice_fusion.6
  51.1 1.1 constant_dynamic-slice_fusion.7
  53.5 1.1 fusion.79
  54.6 1.2 convolution_add_fusion.3
  55.8 1.1 constant_dynamic-slice_fusion.6
  56.9 1.1 constant_dynamic-slice_fusion.7
  59.3 1.1 fusion.79
  60.5 1.2 convolution_add_fusion.3
  62.8 1.1 constant_dynamic-slice_fusion.7
  65.2 1.1 fusion.79
  66.3 1.2 convolution_add_fusion.3
  69.9 33.1 %all-gather = f32[64,128]{1,0:T(8,128)S(1)} all-gather(f32[8,128]{1,0:T(8,128)S(1)} %exp.52), channel_id=2, replica_groups=mesh['sp'=8,'tp'=4] {'sp'}, dimensions={0}, use_global_device_ids=true | all-gather | bytes 36864 | tf_op jit(solution)/shard_map/all_gather | solution.py:14
  103.9 3.6 %exponential_multiply_fusion = f32[8,8,64,128]{3,1,2,0:T(8,128)S(1)} fusion(f32[8,8,64,128]{3,1,2,0:T(8,128)} %get-tuple-element.375, f32[8,8,128]{2,1,0:T(8,128)S(1)} %fusion.52, f32[8,64,8,128]{3,2,1,0:T(8,128)} %bitcast.175), kind=kLoop, calls=%fused_computation.69 | loop fusion | flops 3670016 | bytes 6324224 | tf_op jit(solution)/shard_map/mul | solution.py:121
  107.5 36.7 %all-gather.7.cloned.1.call-done = f32[64,128,128]{2,1,0:T(8,128)} async-done(((f32[8,128,128]{2,1,0:T(8,128)}), f32[64,128,128]{2,1,0:T(8,128)}) %all-gather.7.cloned.1.call-update) | async-done | bytes 4194320 | tf_op jit(solution)/shard_map/all_gather | solution.py:14
  144.2 11.6 %while.28 = (s32[]{:T(128)}, f32[8,128,128]{2,1,0:T(8,128)S(1)}, s32[]{:T(128)}, f32[8,8,128]{2,1,0:T(8,128)S(1)}, f32[8,8,128,128]{3,2,1,0:T(8,128)}, /*index=5*/s32[]{:T(128)}, s32[]{:T(128)}) while((s32[]{:T(128)}, f32[8,128,128]{2,1,0:T(8,128)S(1)}, s32[]{:T(128)}, f32[8,8,128]{2,1,0:T(8,128)S(1)}, ...), condition=%wide.region_5.6_spmd.clone, body=%wide.region_4.5_spmd.clone.sunk | while | flops 524292 | bytes 1585257 | solution.py:26
  144.2 1.4 fusion.80
  145.6 1.4 fusion.80
  147.0 1.4 fusion.80
  148.5 1.4 fusion.80
  149.9 1.4 fusion.80
  151.3 1.4 fusion.80
  152.8 1.5 fusion.80
  154.3 1.5 fusion.80
  155.8 4.7 %multiply_reduce_fusion = (f32[8,64,8]{1,0,2:T(8,128)S(1)}, f32[8,64,8,128]{3,1,0,2:T(8,128)}) fusion(f32[8,8,64,128]{3,2,0,1:T(8,128)} %get-tuple-element.137, f32[8,8,64,128]{3,1,2,0:T(8,128)S(1)} %exponential_multiply_fusion, f32[8,128,128]{2,1,0:T(8,128)S(1)} %get-tuple-element.139), kind=kOutput, calls=%fused_computation.68 | convolution fusion | flops 806875136 | bytes 6832128 | tf_op jit(solution)/shard_map/nhtd,hde->nhte/dot_general | solution.py:122
  160.6 2.8 copy.32
  164.6 1.3 fusion.45
  166.0 14.2 %collective-permute-done = bf16[512,1024]{1,0:T(8,128)(2,1)S(1)} collective-permute-done((bf16[512,1024]{1,0:T(8,128)(2,1)S(1)}, bf16[512,1024]{1,0:T(8,128)(2,1)S(1)}, u32[]{:S(2)}, u32[]{:S(2)}) %collective-permute-start) | collective-permute-done | bytes 1048608 | tf_op jit(solution)/shard_map/ppermute | solution.py:129
  180.2 14.2 %collective-permute-done.1 = bf16[512,1024]{1,0:T(8,128)(2,1)S(1)} collective-permute-done((bf16[512,1024]{1,0:T(8,128)(2,1)S(1)}, bf16[512,1024]{1,0:T(8,128)(2,1)S(1)}, u32[]{:S(2)}, u32[]{:S(2)}) %collective-permute-start.1) | collective-permute-done | bytes 1048608 | tf_op jit(solution)/shard_map/ppermute | solution.py:129
  194.4 14.3 %collective-permute-done.2 = bf16[512,1024]{1,0:T(8,128)(2,1)} collective-permute-done((bf16[512,1024]{1,0:T(8,128)(2,1)S(1)}, bf16[512,1024]{1,0:T(8,128)(2,1)}, u32[]{:S(2)}, u32[]{:S(2)}) %collective-permute-start.2) | collective-permute-done | bytes 1048608 | tf_op jit(solution)/shard_map/ppermute | solution.py:129
  208.7 2.3 constant_dynamic-update-slice_fusion.7
  212.1 1.1 constant_dynamic-update-slice_fusion.5
  213.2 1.1 constant_dynamic-update-slice_fusion.4
  214.3 2.3 constant_dynamic-update-slice_fusion.3
  216.6 1.1 constant_dynamic-update-slice_fusion.2
  219.8 49.5 %all-gather.5.cloned.1.call-done = bf16[4096,1024]{1,0:T(8,128)(2,1)} async-done(((bf16[512,1024]{1,0:T(8,128)(2,1)}), bf16[4096,1024]{1,0:T(8,128)(2,1)}) %all-gather.5.cloned.1.call-update) | async-done | bytes 8388624 | tf_op jit(solution)/shard_map/all_gather | solution.py:94
  269.3 9.2 %fusion.49 = bf16[512,1024]{1,0:T(8,128)(2,1)S(1)} fusion(bf16[4096,1024]{1,0:T(8,128)(2,1)} %all-gather.5.cloned.1.call-done, bf16[512,8192]{1,0:T(8,128)(2,1)} %constant_dynamic-update-slice_fusion, s32[]{:T(128)S(6)} %select_n.47), kind=kOutput, calls=%fused_computation.76 | convolution fusion | flops 4295491584 | bytes 13631492 | tf_op jit(solution)/shard_map/dot_general | solution.py:133
  278.8 5.9 %psum.7 = f32[512]{0:T(512)S(1)} all-reduce(f32[512]{0:T(512)S(1)} %fusion.27), channel_id=1, replica_groups=mesh['sp'=8,'tp'=4] {'tp'}, use_global_device_ids=true, to_apply=%region_9.10 | all-reduce | flops 512 | bytes 4096 | tf_op jit(solution)/shard_map/psum | solution.py:135
  284.7 1.4 fusion.30
  (109 shorter events, 22.7 us)
Async XLA Ops:
  6.5 7.4 %copy-start = (f32[4096]{0:T(1024)S(1)}, f32[4096]{0:T(1024)}, u32[]{:S(2)}) copy-start(f32[4096]{0:T(1024)} %param.18) | copy-start | bytes 49156
  6.5 137.6 %all-gather.7.cloned.1.call-start = ((), (), s32[]{:S(2)}) async-start(), calls=%async_computation.1 | async-start | bytes 4718592 | tf_op jit(solution)/shard_map/all_gather | solution.py:14
  8.3 1.8 copy-start.9
  8.3 1.9 copy-start.5
  10.5 1.2 copy-start.6
  11.8 6.2 %copy-start.3 = (f32[64,8,8,128]{3,2,1,0:T(8,128)}, f32[64,8,8,128]{3,2,1,0:T(8,128)S(1)}, u32[]{:S(2)}) copy-start(f32[64,8,8,128]{3,2,1,0:T(8,128)S(1)} %copy.50) | copy-start | bytes 6291460
  14.0 3.9 %copy-start.4 = (f32[64,8,8,128]{3,2,1,0:T(8,128)S(1)}, f32[64,8,8,128]{3,2,1,0:T(8,128)}, u32[]{:S(2)}) copy-start(f32[64,8,8,128]{3,2,1,0:T(8,128)} %copy.48) | copy-start | bytes 6291460
  20.5 82.5 %copy-start.10 = (f32[128]{0:T(128)S(1)}, f32[128]{0:T(128)}, u32[]{:S(2)}) copy-start(f32[128]{0:T(128)} %param.20) | copy-start | bytes 1540
  67.5 0.8 copy-start.2
  68.3 201.0 %all-gather.5.cloned.1.call-start = ((), (), s32[]{:S(2)}) async-start(), calls=%async_computation | async-start | bytes 9437184 | tf_op jit(solution)/shard_map/all_gather | solution.py:94
  163.4 1.2 copy-start.8
  165.9 14.3 %collective-permute-start = (bf16[512,1024]{1,0:T(8,128)(2,1)S(1)}, bf16[512,1024]{1,0:T(8,128)(2,1)S(1)}, u32[]{:S(2)}, u32[]{:S(2)}) collective-permute-start(bf16[512,1024]{1,0:T(8,128)(2,1)S(1)} %fusion.45), channel_id=1, source_target_pairs={{0,1},{1,2},{2,3},{3,0},{4,5},{5,6},{6,7},{7,4},{8,9},{9,10},{10,1... | collective-permute-start | bytes 3145736 | tf_op jit(solution)/shard_map/ppermute | solution.py:129
  180.2 14.2 %collective-permute-start.1 = (bf16[512,1024]{1,0:T(8,128)(2,1)S(1)}, bf16[512,1024]{1,0:T(8,128)(2,1)S(1)}, u32[]{:S(2)}, u32[]{:S(2)}) collective-permute-start(bf16[512,1024]{1,0:T(8,128)(2,1)S(1)} %collective-permute-done), channel_id=1, source_target_pairs={{0,1},{1,2},{2,3},{3,0},{4,5},{5,6},{6,7},{7,4},{8,9},{9,10},{10,1... | collective-permute-start | bytes 3145736 | tf_op jit(solution)/shard_map/ppermute | solution.py:129
  194.4 14.3 %collective-permute-start.2 = (bf16[512,1024]{1,0:T(8,128)(2,1)S(1)}, bf16[512,1024]{1,0:T(8,128)(2,1)}, u32[]{:S(2)}, u32[]{:S(2)}) collective-permute-start(bf16[512,1024]{1,0:T(8,128)(2,1)S(1)} %collective-permute-done.1), channel_id=1, source_target_pairs={{0,1},{1,2},{2,3},{3,0},{4,5},{5,6},{6,7},{7,4},{8,9},{9,10},{10,1... | collective-permute-start | bytes 3145736 | tf_op jit(solution)/shard_map/ppermute | solution.py:129
  219.8 64.8 %copy-start.7 = (bf16[512,1024]{1,0:T(8,128)(2,1)S(1)}, bf16[512,1024]{1,0:T(8,128)(2,1)}, u32[]{:S(2)}) copy-start(bf16[512,1024]{1,0:T(8,128)(2,1)} %param.23) | copy-start | bytes 3145732
  219.8 64.8 %dynamic-slice-start = ((f32[4096]{0:T(1024)}, s32[]{:T(128)}), f32[1024]{0:T(1024)S(1)}, s32[]{:S(2)}) async-start(f32[4096]{0:T(1024)} %param.22, s32[]{:T(128)} %select_n.45), calls=%async_computation.2 | async-start | bytes 8704 | tf_op jit(solution)/shard_map/dynamic_slice | solution.py:138
  269.3 16.7 %copy-start.1 = (f32[4096]{0:T(1024)S(1)}, f32[4096]{0:T(1024)}, u32[]{:S(2)}) copy-start(f32[4096]{0:T(1024)} %param.18) | copy-start | bytes 49156
Sparse Core Ops, SparseCore 0:
  68.4 75.6 all-gather.6
  146.3 122.9 all-gather.4
